TPU v7x, 768 devices: a whole 4x8x12 slice. The times are simulated.
768 devices in a mesh: ep: 24 (over z, core), tp: 32 (over y, x).
Axes of the slice: x: 4, y: 8, z: 12, core: 2. Of those that a mesh axis runs over, the one named last changes fastest.
Arguments:
- tokens: bfloat16 [768, 4096], P('ep'), may hold values from -6 to 6
- norm_gains: float32 [4, 4096], replicated, may hold values from 0.1 to 1.9
- w_query: bfloat16 [4096, 4096], P(None, 'tp'), may hold values from -0.09375 to 0.09375
- w_query_rope: bfloat16 [4096, 2048], P(None, 'tp'), may hold values from -0.09375 to 0.09375
- w_key_up: bfloat16 [32, 128, 1024], P('tp'), may hold values from -0.5 to 0.5
- w_value_up: bfloat16 [32, 1024, 128], P('tp'), may hold values from -0.1875 to 0.1875
- w_output: bfloat16 [4096, 4096], P('tp'), may hold values from -0.09375 to 0.09375
- w_latent_down: bfloat16 [4096, 1024], P(None, 'tp'), may hold values from -0.09375 to 0.09375
- latent_gain: float32 [1024], replicated, may hold values from 0.1 to 1.9
- w_rope_down: bfloat16 [4096, 64], replicated, may hold values from -0.09375 to 0.09375
- cache_latent: bfloat16 [768, 1024, 1024], P(('ep', 'tp')), may hold values from -300 to 300
- cache_rope: bfloat16 [768, 1024, 64], P(('ep', 'tp')), may hold values from -6 to 6
- lengths: int32 [768], P(('ep', 'tp')), may hold values from 1 to 1024, as said below
- routes: int32 [768, 2], P('ep'), may hold values from 0 to 23, all different within a row; in each aligned block of 32 rows (0 to 31, 32 to 63, ...) at most 5 rows name the same one
- route_weights: float32 [768, 2], P('ep'), may hold values from 0.2 to 1
- w_gate: bfloat16 [24, 4096, 2048], P('ep', None, 'tp'), may hold values from -0.09375 to 0.09375
- w_up: bfloat16 [24, 4096, 2048], P('ep', None, 'tp'), may hold values from -0.09375 to 0.09375
- w_down: bfloat16 [24, 2048, 4096], P('ep', 'tp'), may hold values from -0.125 to 0.125
Outputs:
- hidden_out: bfloat16 [768, 4096], P(('ep', 'tp'))
- new_latent: bfloat16 [768, 1024], P(('ep', 'tp'))
- new_rope: bfloat16 [768, 64], P(('ep', 'tp'))
Inputs may be any that keep to these rules, and one draw needn't show every extreme that they name: `routes`: within each aligned block of 32 rows no expert is named by more than 5 rows, a bound that some block reaches; the 2 experts of a row differ. The new token stands at position lengths; some sequence has exactly 1024.
All inputs are finite; a program needn't handle non-finite values.
Results may differ from a plain program's by a relative error of at most 0.02.
Values may be sent and summed in bfloat16 or wider, within the bound.
A program may use at most 32 MiB of HBM per device.

v0:
```python
import jax
import jax.numpy as jnp
from jax import lax
from jax.sharding import PartitionSpec as P

EXP_LOCAL = 1


EPSILON = 1e-06
ROTARY_BASE = 500000.0


def in_blocks(value, dim, count):
    dims = value.shape
    blocks = value.reshape(*dims[:dim], count, dims[dim] // count, *dims[dim + 1 :])
    return jnp.moveaxis(blocks, dim, 0)


def sum_at_owner(value, axis, dim):
    count = lax.axis_size(axis)
    blocks = lax.all_to_all(in_blocks(value, dim, count), axis, 0, 0, tiled=True)
    return jnp.sum(blocks.astype(jnp.float32), axis=0)


def copy_for_each(value, axis):
    copies = jnp.broadcast_to(value, (lax.axis_size(axis), *value.shape))
    return lax.all_to_all(copies, axis, split_axis=0, concat_axis=0, tiled=True)


def in_order(blocks, dim):
    dims = list(blocks.shape[1:])
    dims[dim] *= blocks.shape[0]
    return jnp.moveaxis(blocks, 0, dim).reshape(dims)


def collect(value, axis, dim):
    blocks = copy_for_each(value, axis)
    return in_order(blocks, dim)


def rms_scale(source, gain_row):
    values_f = source.astype(jnp.float32)
    return (
        values_f
        * lax.rsqrt(jnp.mean(values_f * values_f, axis=-1, keepdims=True) + EPSILON)
        * gain_row
    )


def rotate(source, position):
    half_width = source.shape[-1] // 2
    frequency = ROTARY_BASE ** (-jnp.arange(half_width, dtype=jnp.float32) / half_width)
    angles = position[..., None] * frequency
    first_half = source[..., :half_width]
    second_half = source[..., half_width:]
    return jnp.concatenate(
        [
            first_half * jnp.cos(angles) - second_half * jnp.sin(angles),
            second_half * jnp.cos(angles) + first_half * jnp.sin(angles),
        ],
        axis=-1,
    )


def attend(q_latent, q_pe, cache_lat, cache_rp, lat_new, rope_new, lengths, score_scale):
    scores = (
        jnp.einsum("shc,spc->shp", q_latent, cache_lat, preferred_element_type=jnp.float32)
        + jnp.einsum("shr,spr->shp", q_pe, cache_rp, preferred_element_type=jnp.float32)
    ) * score_scale
    own_score = (
        jnp.einsum("shc,sc->sh", q_latent, lat_new, preferred_element_type=jnp.float32)
        + jnp.einsum("shr,sr->sh", q_pe, rope_new, preferred_element_type=jnp.float32)
    ) * score_scale
    visible = (
        jnp.arange(cache_lat.shape[1], dtype=jnp.int32)[None, None, :] < lengths[:, None, None]
    )
    row_max = jnp.maximum(jnp.max(jnp.where(visible, scores, -jnp.inf), axis=-1), own_score)
    weights = jnp.where(visible, jnp.exp(scores - row_max[..., None]), 0.0)
    own_weight = jnp.exp(own_score - row_max)
    denominator = jnp.sum(weights, axis=-1) + own_weight
    probabilities = (weights / denominator[..., None]).astype(jnp.bfloat16)
    own_prob = (own_weight / denominator).astype(jnp.bfloat16)
    attended = jnp.einsum(
        "shp,spc->shc", probabilities, cache_lat, preferred_element_type=jnp.float32
    )
    attended = (
        attended + own_prob.astype(jnp.float32)[..., None] * lat_new.astype(jnp.float32)[:, None, :]
    )
    return attended.astype(jnp.bfloat16)


def on_device(
    tokens,
    norm_gains,
    w_query,
    w_query_rope,
    w_key_up,
    w_value_up,
    w_output,
    w_latent_down,
    latent_gain,
    w_rope_down,
    cache_latent,
    cache_rope,
    lengths,
    routes,
    route_weights,
    w_gate,
    w_up,
    w_down,
):
    group_rows = tokens.shape[0]
    seq_count = cache_latent.shape[0]
    heads_here = w_key_up.shape[0]
    nope_width = w_key_up.shape[1]
    rope_width = w_rope_down.shape[1]
    tp_size = lax.axis_size("tp")
    tp_rank = lax.axis_index("tp")
    normed = rms_scale(tokens, norm_gains[0]).astype(jnp.bfloat16)
    q_nope = jnp.dot(normed, w_query, preferred_element_type=jnp.float32).astype(jnp.bfloat16)
    q_nope = q_nope.reshape(group_rows, heads_here, nope_width)
    q_latent = jnp.einsum("thn,hnc->thc", q_nope, w_key_up, preferred_element_type=jnp.float32)
    q_latent = q_latent.astype(jnp.bfloat16).reshape(group_rows, -1)
    q_rot = jnp.dot(normed, w_query_rope, preferred_element_type=jnp.float32).astype(jnp.bfloat16)
    latent_cols = jnp.dot(normed, w_latent_down, preferred_element_type=jnp.float32).astype(
        jnp.bfloat16
    )
    q_mine, rot_mine, latent_raw = (
        lax.all_to_all(q_latent, "tp", split_axis=0, concat_axis=1, tiled=True),
        lax.all_to_all(q_rot, "tp", split_axis=0, concat_axis=1, tiled=True),
        lax.all_to_all(latent_cols, "tp", split_axis=0, concat_axis=1, tiled=True),
    )
    heads_all = rot_mine.shape[1] // rope_width
    own_normed = lax.dynamic_slice_in_dim(normed, tp_rank * seq_count, seq_count, 0)
    rope_raw = jnp.dot(own_normed, w_rope_down, preferred_element_type=jnp.float32).astype(
        jnp.bfloat16
    )
    new_latent = rms_scale(latent_raw, latent_gain).astype(jnp.bfloat16)
    position = lengths.astype(jnp.float32)
    new_rope = rotate(rope_raw.astype(jnp.float32), position).astype(jnp.bfloat16)
    q_pe = rotate(
        rot_mine.reshape(seq_count, heads_all, rope_width).astype(jnp.float32), position[:, None]
    )
    q_pe = q_pe.astype(jnp.bfloat16)
    score_scale = (nope_width + rope_width) ** (-0.5)
    attended = attend(
        q_mine.reshape(seq_count, heads_all, -1),
        q_pe,
        cache_latent,
        cache_rope,
        new_latent,
        new_rope,
        lengths,
        score_scale,
    )
    head_latent = lax.all_to_all(
        attended.reshape(seq_count, -1), "tp", split_axis=1, concat_axis=0, tiled=True
    )
    values = (
        jnp.einsum(
            "thc,hcv->thv",
            head_latent.reshape(group_rows, heads_here, -1),
            w_value_up,
            preferred_element_type=jnp.float32,
        )
        .astype(jnp.bfloat16)
        .reshape(group_rows, -1)
    )
    head_term = jnp.dot(values, w_output, preferred_element_type=jnp.float32)
    mixed_own = sum_at_owner(head_term.astype(jnp.bfloat16), "tp", 0)
    own_tokens = lax.dynamic_slice_in_dim(tokens, tp_rank * seq_count, seq_count, 0)
    own_resid = (own_tokens.astype(jnp.float32) + rms_scale(mixed_own, norm_gains[1])).astype(
        jnp.bfloat16
    )
    own_expert_in = rms_scale(own_resid, norm_gains[2]).astype(jnp.bfloat16)
    expert_in = collect(own_expert_in, "tp", 0)
    ep_size = lax.axis_size("ep")
    experts = ep_size * EXP_LOCAL
    local_expert = tp_rank // (tp_size // EXP_LOCAL)
    route_count = routes.shape[1]
    capacity = (
        (group_rows * route_count + experts - 1) // experts
        + 2
        + group_rows * route_count // (4 * experts)
    )
    slot_count = ep_size * capacity
    flat_routes = routes.reshape(-1)
    expert_hits = (flat_routes[:, None] == jnp.arange(experts, dtype=jnp.int32)[None, :]).astype(
        jnp.int32
    )
    slot_rank = jnp.sum((jnp.cumsum(expert_hits, axis=0) - 1) * expert_hits, axis=1)
    served_here = flat_routes % EXP_LOCAL == local_expert
    slot_index = jnp.where(served_here, flat_routes // EXP_LOCAL * capacity + slot_rank, -1)
    slot_picks = (slot_index[:, None] == jnp.arange(slot_count, dtype=jnp.int32)[None, :]).astype(
        jnp.bfloat16
    )
    slot_picks = slot_picks.reshape(group_rows, route_count, slot_count)
    slot_rows = jnp.sum(slot_picks, axis=1)
    outgoing = jnp.dot(slot_rows.T, expert_in, preferred_element_type=jnp.float32).astype(
        jnp.bfloat16
    )
    arrived = lax.all_to_all(outgoing, "ep", split_axis=0, concat_axis=0, tiled=True)
    gate_sum = jnp.dot(arrived, w_gate[0], preferred_element_type=jnp.float32)
    up_sum = jnp.dot(arrived, w_up[0], preferred_element_type=jnp.float32)
    hidden_units = (jax.nn.silu(gate_sum) * up_sum).astype(jnp.bfloat16)
    expert_out = jnp.dot(hidden_units, w_down[0], preferred_element_type=jnp.float32).astype(
        jnp.bfloat16
    )
    returned = lax.all_to_all(expert_out, "ep", split_axis=0, concat_axis=0, tiled=True)
    routed_part = jnp.zeros((group_rows, returned.shape[1]), jnp.float32)
    for route_slot in range(route_count):
        chosen = jnp.dot(slot_picks[:, route_slot, :], returned, preferred_element_type=jnp.float32)
        routed_part = routed_part + route_weights[:, route_slot : route_slot + 1] * chosen
    routed = sum_at_owner(routed_part.astype(jnp.bfloat16), "tp", 0)
    hidden_out = (own_resid.astype(jnp.float32) + rms_scale(routed, norm_gains[3])).astype(
        jnp.bfloat16
    )
    return (hidden_out, new_latent, new_rope)


def solution(mesh):
    in_specs = (
        P("ep", None),
        P(),
        P(None, "tp"),
        P(None, "tp"),
        P("tp", None, None),
        P("tp", None, None),
        P("tp", None),
        P(None, "tp"),
        P(),
        P(),
        P(("ep", "tp"), None, None),
        P(("ep", "tp"), None, None),
        P(("ep", "tp")),
        P("ep", None),
        P("ep", None),
        P("ep", None, "tp"),
        P("ep", None, "tp"),
        P("ep", "tp", None),
    )
    out_specs = (P(("ep", "tp"), None), P(("ep", "tp"), None), P(("ep", "tp"), None))
    return jax.shard_map(
        on_device, mesh=mesh, in_specs=in_specs, out_specs=out_specs, check_vma=False
    )
```

profile of v0, /device:TPU:1, one launch (start us, length us, event | category | flops | bytes accessed | tf_op | source)
XLA Modules:
  0.0 286.0 jit_solution(18275850269827072888)
XLA Ops:
  0.7 1.0 slice.36
  1.7 1.1 fusion.27
  2.8 1.1 fusion.29
  3.9 1.2 fusion.21
  5.0 0.6 copy.50
  5.7 10.5 %all-to-all-start.2 = ((bf16[32,1,32]{2,1,0:T(2,128)(2,1)}), bf16[32,1,32]{2,1,0:T(2,128)(2,1)S(1)}, u32[]{:S(2)}, u32[]{:S(2)}) async-start(bf16[32,1,32]{2,1,0:T(2,128)(2,1)} %copy.50), calls=%async_computation.2 | async-start | bytes 32768 | tf_op jit(solution)/shard_map/all_to_all | solution.py:131
  16.2 1.3 fusion.20
  18.7 1.3 fusion.26
  20.1 1.4 fusion.15
  21.5 0.6 copy.49
  22.6 0.7 reduce.19
  23.3 0.7 reshape.414
  23.9 0.9 all-to-all-done.2
  24.8 8.4 %all-to-all-start.1 = ((bf16[32,1,64]{2,1,0:T(2,128)(2,1)}), bf16[32,1,64]{2,1,0:T(2,128)(2,1)S(1)}, u32[]{:S(2)}, u32[]{:S(2)}) async-start(bf16[32,1,64]{2,1,0:T(2,128)(2,1)} %copy.49), calls=%async_computation.1 | async-start | bytes 32768 | tf_op jit(solution)/shard_map/all_to_all | solution.py:130
  33.2 0.6 multiply_reduce_fusion.4
  34.7 7.0 %all-to-all-done.1 = bf16[32,1,64]{2,1,0:T(2,128)(2,1)S(1)} async-done(((bf16[32,1,64]{2,1,0:T(2,128)(2,1)}), bf16[32,1,64]{2,1,0:T(2,128)(2,1)S(1)}, u32[]{:S(2)}, u32[]{:S(2)}) %all-to-all-start.1) | async-done | bytes 4128 | tf_op jit(solution)/shard_map/all_to_all | solution.py:130
  41.7 3.9 %all-to-all-start = ((bf16[32,2,512]{2,1,0:T(2,128)(2,1)}), bf16[32,2,512]{2,1,0:T(2,128)(2,1)S(1)}, u32[]{:S(2)}, u32[]{:S(2)}) async-start(bf16[32,2,512]{2,1,0:T(2,128)(2,1)} %reshape.414), calls=%async_computation | async-start | bytes 131072 | tf_op jit(solution)/shard_map/all_to_all | solution.py:129
  45.6 0.7 fusion.63
  46.3 8.2 %all-to-all-done = bf16[32,2,512]{2,1,0:T(2,128)(2,1)S(1)} async-done(((bf16[32,2,512]{2,1,0:T(2,128)(2,1)}), bf16[32,2,512]{2,1,0:T(2,128)(2,1)S(1)}, u32[]{:S(2)}, u32[]{:S(2)}) %all-to-all-start) | async-done | bytes 65568 | tf_op jit(solution)/shard_map/all_to_all | solution.py:129
  54.5 0.7 fusion.6
  56.8 1.0 reduce.20
  57.8 11.8 %all_to_all.88 = bf16[32,2,512]{2,1,0:T(2,128)(2,1)S(1)} all-to-all(bf16[32,2,512]{2,1,0:T(2,128)(2,1)S(1)} %reshape.416), channel_id=1, replica_groups=mesh['ep'=24,'tp'=32] {'tp'}, dimensions={0} | all-to-all | bytes 131072 | tf_op jit(solution)/shard_map/all_to_all | solution.py:156
  69.7 1.4 fusion.2
  71.1 0.8 reduce.21
  71.9 0.9 reshape.418
  72.8 3.9 %all-to-all-start.4 = ((bf16[32,2,2048]{2,1,0:T(2,128)(2,1)}), bf16[32,2,2048]{2,1,0:T(2,128)(2,1)S(1)}, u32[]{:S(2)}, u32[]{:S(2)}) async-start(bf16[32,2,2048]{2,1,0:T(2,128)(2,1)} %reshape.418), calls=%async_computation.4 | async-start | bytes 524288 | tf_op jit(solution)/shard_map/all_to_all | solution.py:21
  76.9 10.4 %all-to-all-done.4 = bf16[32,2,2048]{2,1,0:T(2,128)(2,1)S(1)} async-done(((bf16[32,2,2048]{2,1,0:T(2,128)(2,1)}), bf16[32,2,2048]{2,1,0:T(2,128)(2,1)S(1)}, u32[]{:S(2)}, u32[]{:S(2)}) %all-to-all-start.4) | async-done | bytes 262176 | tf_op jit(solution)/shard_map/all_to_all | solution.py:21
  89.4 1.5 multiply_reduce_fusion.1
  92.1 2.2 reduce.22
  94.3 0.9 reshape.420
  95.2 3.9 %all-to-all-start.5 = ((bf16[32,2,2048]{2,1,0:T(2,128)(2,1)}), bf16[32,2,2048]{2,1,0:T(2,128)(2,1)S(1)}, u32[]{:S(2)}, u32[]{:S(2)}) async-start(bf16[32,2,2048]{2,1,0:T(2,128)(2,1)} %reshape.420), calls=%async_computation.5 | async-start | bytes 524288 | tf_op jit(solution)/shard_map/all_to_all | solution.py:27
  99.7 9.9 %all-to-all-done.5 = bf16[32,2,2048]{2,1,0:T(2,128)(2,1)S(1)} async-done(((bf16[32,2,2048]{2,1,0:T(2,128)(2,1)}), bf16[32,2,2048]{2,1,0:T(2,128)(2,1)S(1)}, u32[]{:S(2)}, u32[]{:S(2)}) %all-to-all-start.5) | async-done | bytes 262176 | tf_op jit(solution)/shard_map/all_to_all | solution.py:27
  109.6 1.0 reshape.421
  110.6 1.5 convolution_convert_fusion.1
  112.1 1.5 all_to_all.72
  113.6 78.6 %all_to_all.89 = bf16[24,5,4096]{2,1,0:T(8,128)(2,1)} all-to-all(bf16[24,5,4096]{2,1,0:T(8,128)(2,1)} %all_to_all.72), channel_id=1, replica_groups=mesh['ep'=24,'tp'=32] {'ep'}, dimensions={0} | all-to-all | bytes 1966080 | tf_op jit(solution)/shard_map/all_to_all | solution.py:202
  192.2 1.7 all_to_all.74
  193.9 1.5 fusion.33
  195.5 3.5 %convolution_convert_fusion = bf16[120,4096]{1,0:T(8,128)(2,1)} fusion(bf16[120,4096]{1,0:T(8,128)(2,1)S(1)} %all_to_all.74, bf16[1,64,4096]{2,1,0:T(8,128)(2,1)} %param.35, bf16[1,4096,64]{1,2,0:T(8,128)(2,1)} %param.34, f32[120,64]{0,1:T(8,128)S(1)} %fusion.33), kind=kOutput, calls=%fused_computation | convolution fusion | flops 126366720 | bytes 3045376 | tf_op jit(solution)/shard_map/dot_general | solution.py:206
  198.9 2.5 all_to_all.75
  201.4 6.9 %all-to-all-start.7 = ((bf16[24,5,4096]{2,1,0:T(8,128)(2,1)}), bf16[24,5,4096]{2,1,0:T(8,128)(2,1)}, u32[]{:S(2)}, u32[]{:S(2)}) async-start(bf16[24,5,4096]{2,1,0:T(8,128)(2,1)} %all_to_all.75), calls=%async_computation.7 | async-start | bytes 3145728 | tf_op jit(solution)/shard_map/all_to_all | solution.py:209
  208.5 56.4 %all-to-all-done.7 = bf16[24,5,4096]{2,1,0:T(8,128)(2,1)} async-done(((bf16[24,5,4096]{2,1,0:T(8,128)(2,1)}), bf16[24,5,4096]{2,1,0:T(8,128)(2,1)}, u32[]{:S(2)}, u32[]{:S(2)}) %all-to-all-start.7) | async-done | bytes 983072 | tf_op jit(solution)/shard_map/all_to_all | solution.py:209
  264.9 1.7 all_to_all.77
  267.2 0.8 reduce.23
  268.0 0.9 reshape.422
  268.9 3.9 %all-to-all-start.8 = ((bf16[32,2,2048]{2,1,0:T(2,128)(2,1)}), bf16[32,2,2048]{2,1,0:T(2,128)(2,1)S(1)}, u32[]{:S(2)}, u32[]{:S(2)}) async-start(bf16[32,2,2048]{2,1,0:T(2,128)(2,1)} %reshape.422), calls=%async_computation.8 | async-start | bytes 524288 | tf_op jit(solution)/shard_map/all_to_all | solution.py:21
  273.9 9.3 %all-to-all-done.8 = bf16[32,2,2048]{2,1,0:T(2,128)(2,1)S(1)} async-done(((bf16[32,2,2048]{2,1,0:T(2,128)(2,1)}), bf16[32,2,2048]{2,1,0:T(2,128)(2,1)S(1)}, u32[]{:S(2)}, u32[]{:S(2)}) %all-to-all-start.8) | async-done | bytes 262176 | tf_op jit(solution)/shard_map/all_to_all | solution.py:21
  285.3 0.6 add_convert_fusion
  (61 shorter events, 9.0 us)
Async XLA Ops:
  0.6 53.9 %copy-start = (bf16[1,1024,1024]{2,1,0:T(8,128)(2,1)S(1)}, bf16[1,1024,1024]{2,1,0:T(8,128)(2,1)}, u32[]{:S(2)}) copy-start(bf16[1,1024,1024]{2,1,0:T(8,128)(2,1)} %param.28) | copy-start | bytes 6291460
  0.6 19.4 %copy-start.1 = (bf16[4096,128]{1,0:T(8,128)(2,1)S(1)}, bf16[4096,128]{1,0:T(8,128)(2,1)}, u32[]{:S(2)}) copy-start(bf16[4096,128]{1,0:T(8,128)(2,1)} %param.20) | copy-start | bytes 3145732
  3.9 30.8 %copy-start.5 = (f32[1024]{0:T(1024)S(1)}, f32[1024]{0:T(1024)}, u32[]{:S(2)}) copy-start(f32[1024]{0:T(1024)} %param.26) | copy-start | bytes 12292
  5.7 19.1 %all-to-all-start.2 = ((bf16[32,1,32]{2,1,0:T(2,128)(2,1)}), bf16[32,1,32]{2,1,0:T(2,128)(2,1)S(1)}, u32[]{:S(2)}, u32[]{:S(2)}) async-start(bf16[32,1,32]{2,1,0:T(2,128)(2,1)} %copy.50), calls=%async_computation.2 | async-start | bytes 32768 | tf_op jit(solution)/shard_map/all_to_all | solution.py:131
  24.8 16.9 %all-to-all-start.1 = ((bf16[32,1,64]{2,1,0:T(2,128)(2,1)}), bf16[32,1,64]{2,1,0:T(2,128)(2,1)S(1)}, u32[]{:S(2)}, u32[]{:S(2)}) async-start(bf16[32,1,64]{2,1,0:T(2,128)(2,1)} %copy.49), calls=%async_computation.1 | async-start | bytes 32768 | tf_op jit(solution)/shard_map/all_to_all | solution.py:130
  34.6 20.8 %copy-start.3 = (bf16[1,1024,64]{1,2,0:T(8,128)(2,1)S(1)}, bf16[1,1024,64]{1,2,0:T(8,128)(2,1)}, u32[]{:S(2)}) copy-start(bf16[1,1024,64]{1,2,0:T(8,128)(2,1)} %param.29) | copy-start | bytes 393220
  41.7 12.7 %all-to-all-start = ((bf16[32,2,512]{2,1,0:T(2,128)(2,1)}), bf16[32,2,512]{2,1,0:T(2,128)(2,1)S(1)}, u32[]{:S(2)}, u32[]{:S(2)}) async-start(bf16[32,2,512]{2,1,0:T(2,128)(2,1)} %reshape.414), calls=%async_computation | async-start | bytes 131072 | tf_op jit(solution)/shard_map/all_to_all | solution.py:129
  55.2 14.5 %copy-start.2 = (bf16[128,4096]{1,0:T(8,128)(2,1)S(1)}, bf16[128,4096]{1,0:T(8,128)(2,1)}, u32[]{:S(2)}) copy-start(bf16[128,4096]{1,0:T(8,128)(2,1)} %param.24) | copy-start | bytes 3145732
  56.7 20.0 %copy-start.6 = (s32[32,2]{0,1:T(2,128)S(1)}, s32[32,2]{0,1:T(2,128)}, u32[]{:S(2)}) copy-start(s32[32,2]{0,1:T(2,128)} %param.31) | copy-start | bytes 772
  71.1 18.3 %copy-start.4 = (f32[4,4096]{1,0:T(4,128)S(1)}, f32[4,4096]{1,0:T(4,128)}, u32[]{:S(2)}) copy-start(f32[4,4096]{1,0:T(4,128)} %param.19) | copy-start | bytes 196612
  72.8 14.4 %all-to-all-start.4 = ((bf16[32,2,2048]{2,1,0:T(2,128)(2,1)}), bf16[32,2,2048]{2,1,0:T(2,128)(2,1)S(1)}, u32[]{:S(2)}, u32[]{:S(2)}) async-start(bf16[32,2,2048]{2,1,0:T(2,128)(2,1)} %reshape.418), calls=%async_computation.4 | async-start | bytes 524288 | tf_op jit(solution)/shard_map/all_to_all | solution.py:21
  95.2 14.4 %all-to-all-start.5 = ((bf16[32,2,2048]{2,1,0:T(2,128)(2,1)}), bf16[32,2,2048]{2,1,0:T(2,128)(2,1)S(1)}, u32[]{:S(2)}, u32[]{:S(2)}) async-start(bf16[32,2,2048]{2,1,0:T(2,128)(2,1)} %reshape.420), calls=%async_computation.5 | async-start | bytes 524288 | tf_op jit(solution)/shard_map/all_to_all | solution.py:27
  201.4 6.9 %copy-start.7 = (f32[32,2]{0,1:T(2,128)S(1)}, f32[32,2]{0,1:T(2,128)}, u32[]{:S(2)}) copy-start(f32[32,2]{0,1:T(2,128)} %param.32) | copy-start | bytes 772
  201.4 63.5 %all-to-all-start.7 = ((bf16[24,5,4096]{2,1,0:T(8,128)(2,1)}), bf16[24,5,4096]{2,1,0:T(8,128)(2,1)}, u32[]{:S(2)}, u32[]{:S(2)}) async-start(bf16[24,5,4096]{2,1,0:T(8,128)(2,1)} %all_to_all.75), calls=%async_computation.7 | async-start | bytes 3145728 | tf_op jit(solution)/shard_map/all_to_all | solution.py:209
  268.9 14.4 %all-to-all-start.8 = ((bf16[32,2,2048]{2,1,0:T(2,128)(2,1)}), bf16[32,2,2048]{2,1,0:T(2,128)(2,1)S(1)}, u32[]{:S(2)}, u32[]{:S(2)}) async-start(bf16[32,2,2048]{2,1,0:T(2,128)(2,1)} %reshape.422), calls=%async_computation.8 | async-start | bytes 524288 | tf_op jit(solution)/shard_map/all_to_all | solution.py:21
where the time goes:
time: 289 us; the launch traced here: 286 us
  waiting for transfers between devices  102 us (35%)
  blocking collectives  90.4 us (31%)
  starting transfers between devices  41.2 us (14%)
  local copies, waits for them, and re-layouts  16.8 us (6%)
  other arithmetic  15.5 us (5%)
  matrix products  15.5 us (5%)
  between operations  4.49 us (2%)
    all_to_all x1, blocking collectives, on_device(): lax.all_to_all(outgoing, 'ep', split_axis=0, concat_axis=0, tiled=True)  78.6 us
    all_to_all x1, waiting for transfers between devices, on_device(): lax.all_to_all(expert_out, 'ep', split_axis=0, concat_axis=0, tiled=True)  56.4 us
    all_to_all x2, waiting for transfers between devices, sum_at_owner(): lax.all_to_all(in_blocks(value, dim, count), axis, 0, 0, tiled=True)  19.7 us
    all_to_all x1, blocking collectives, on_device(): lax.all_to_all(attended.reshape(seq_count, -1), 'tp', split_axis=1, conca...  11.8 us
    all_to_all x1, starting transfers between devices, on_device(): lax.all_to_all(latent_cols, 'tp', split_axis=0, concat_axis=1, tiled=True)  10.5 us
    all_to_all x1, waiting for transfers between devices, copy_for_each(): return lax.all_to_all(copies, axis, split_axis=0, concat_axis=0, tiled=True)  9.93 us
    all_to_all x1, starting transfers between devices, on_device(): lax.all_to_all(q_rot, 'tp', split_axis=0, concat_axis=1, tiled=True)  8.36 us
    all_to_all x1, waiting for transfers between devices, on_device(): lax.all_to_all(q_latent, 'tp', split_axis=0, concat_axis=1, tiled=True)  8.16 us
  transfers between devices with their start and end apart: 7, of which 7 were waited for; matrix products, arithmetic and copies ran while one was open for 4% of the time, Pallas kernels for 0%

commit v1 on v0

v1 whole, which is shorter than its diff:
```python
import functools
import math

import jax
import jax.numpy as jnp
from jax import lax
from jax.experimental import pallas as pl
from jax.experimental.pallas import tpu as pltpu
from jax.sharding import PartitionSpec as P

EPSILON = 1e-06
ROTARY_BASE = 500000.0
X_SIZE = 4
LANES = 128
CAP = 5
CAP_PAD = 6
BF16 = jnp.bfloat16
F32 = jnp.float32
NT = (((1,), (1,)), ((), ()))


def dot(a, b):
    return jnp.dot(a, b, preferred_element_type=F32)


def dot_nt(a, b):
    return lax.dot_general(a, b, NT, preferred_element_type=F32)


def iota(shape, dim):
    return lax.broadcasted_iota(jnp.int32, shape, dim)


def send_to_all(axis, count, me, source_of, target, send_sem, recv_sem):
    def step(i, carry):
        peer = lax.rem(me + i, count)
        pltpu.make_async_remote_copy(
            src_ref=source_of(peer),
            dst_ref=target,
            send_sem=send_sem,
            recv_sem=recv_sem,
            device_id={axis: peer},
            device_id_type=pl.DeviceIdType.MESH,
        ).start()
        return carry

    lax.fori_loop(1, count, step, 0)


def wait_bytes(ref, sem):
    pltpu.make_async_copy(ref, ref, sem).wait()


def step_kernel(
    n_ep,
    n_tp,
    cap,
    cap_pad,
    score_scale,
    tokens_h,
    gains_h,
    wq_h,
    wqr_h,
    wku_h,
    wvu_h,
    wo_h,
    wld_h,
    lgain_v,
    wrd_h,
    cl_h,
    cr_h,
    len_s,
    routes_v,
    rw_v,
    wg_h,
    wu_h,
    wd_h,
    trig_v,
    out_v,
    nl_v,
    nr_v,
    tok_v,
    gains_v,
    wq_v,
    wside_v,
    wku_v,
    wvu_v,
    wo_v,
    cl_v,
    cr_v,
    wgu_v,
    wd_v,
    load_sem,
    norm_v,
    rows_v,
    scat_v,
    extra1,
    msg1,
    rec1e,
    rec1,
    msg2,
    rec2,
    msg3,
    rec3,
    msg4,
    rec4,
    msg5,
    rec5,
    chunks6,
    msg7,
    rec7,
    msg8,
    rec8,
    msg9,
    rec9,
    pick_v,
    back_v,
    ssem,
    rsem,
    rsem6,
    rsem7,
):
    e = lax.axis_index("ep")
    t = lax.axis_index("tp")
    x = lax.rem(t, X_SIZE)
    y0 = t - x
    rows = tok_v.shape[0]
    nblk = tok_v.shape[1] // LANES
    sub = nblk // X_SIZE
    slots = n_ep * cap_pad
    lat_blk = 8

    loads = [
        (tokens_h, tok_v),
        (gains_h, gains_v),
        (wq_h, wq_v),
        (wqr_h, wside_v.at[0:64]),
        (wrd_h, wside_v.at[64:128]),
        (wld_h, wside_v.at[128 : 128 + wld_h.shape[0]]),
        (wku_h.at[0], wku_v),
        (cl_h.at[0], cl_v),
        (cr_h.at[0], cr_v),
        (wvu_h.at[0], wvu_v),
        (wo_h, wo_v),
        (wg_h.at[0], wgu_v.at[0:64]),
        (wu_h.at[0], wgu_v.at[64:128]),
        (wd_h.at[0], wd_v),
    ]
    copies = [pltpu.make_async_copy(s, d, load_sem.at[i]) for i, (s, d) in enumerate(loads)]
    for c in copies:
        c.start()

    barrier = pltpu.get_barrier_semaphore()

    def greet(axis, count, me):
        def step(i, carry):
            pl.semaphore_signal(
                barrier,
                inc=1,
                device_id={axis: lax.rem(me + i, count)},
                device_id_type=pl.DeviceIdType.MESH,
            )
            return carry

        lax.fori_loop(1, count, step, 0)

    greet("tp", n_tp, t)
    greet("ep", n_ep, e)

    copies[0].wait()
    copies[1].wait()
    tok = tok_v[...].astype(F32)
    scale0 = lax.rsqrt(jnp.mean(tok * tok, axis=-1, keepdims=True) + EPSILON)
    norm_v[...] = (tok * scale0 * gains_v[0:1, :]).astype(BF16)
    copies[2].wait()
    q_nope = dot(norm_v[...], wq_v[...]).astype(BF16)
    copies[6].wait()
    q_lat = dot(q_nope, wku_v[...])
    for j in range(lat_blk):
        scat_v[j * rows : (j + 1) * rows, :] = q_lat[:, j * LANES : (j + 1) * LANES]
    for r in range(rows):
        msg1[r] = scat_v[pl.ds(r, lat_blk, stride=rows), :].astype(BF16)
    for i in (3, 4, 5):
        copies[i].wait()
    side = dot_nt(norm_v[...], wside_v[...]).astype(BF16)
    q_rot = side[:, 0:64]
    rope_all = side[:, 64:128].astype(F32)
    cols = wld_h.shape[0]
    per_row = LANES // cols
    lat_cols = side[:, 128 : 128 + cols]
    place = (iota((cols, LANES), 1) == iota((cols, LANES), 0) + cols * lax.rem(t, per_row)).astype(F32).astype(BF16)
    widen = (iota((64, LANES), 1) == iota((64, LANES), 0)).astype(F32).astype(BF16)
    extra1[:, 0, 0:LANES] = dot(q_rot, widen)
    extra1[:, 0, LANES : 2 * LANES] = dot(lat_cols, place)
    rec1[t] = msg1[t]
    rec1e[t] = extra1[t]

    pl.semaphore_wait(barrier, n_tp - 1 + n_ep - 1)
    send_to_all("tp", n_tp, t, lambda p: msg1.at[p], rec1.at[t], ssem.at[0], rsem.at[0])
    send_to_all("tp", n_tp, t, lambda p: extra1.at[p], rec1e.at[t], ssem.at[1], rsem.at[1])

    own_row = (iota((rows, 64), 0) == t).astype(F32)
    rope_raw = jnp.sum(rope_all * own_row, axis=0, keepdims=True)
    cos = trig_v[0:1, 0:64]
    sin = trig_v[1:2, 0:64]
    swap64 = (lax.rem(iota((64, 64), 0) + 32, 64) == iota((64, 64), 1)).astype(F32).astype(BF16)

    def rotated(v):
        return v * cos + dot(v.astype(BF16), swap64) * sin

    rope8 = jnp.broadcast_to(rope_raw, (8, 64))
    new_rope = rotated(rope8)[0:1].astype(BF16)
    nr_v[...] = new_rope

    own_tok = jnp.sum(jnp.where(iota(tok.shape, 0) == t, tok, 0.0), axis=0, keepdims=True)
    for b in range(nblk):
        rows_v[0, b : b + 1, :] = own_tok[:, b * LANES : (b + 1) * LANES]
        for g in range(1, 4):
            rows_v[g, b : b + 1, :] = gains_v[g : g + 1, b * LANES : (b + 1) * LANES]

    routes = routes_v[...].astype(F32)
    upper = (iota((rows, rows), 0) < iota((rows, rows), 1)).astype(F32)
    experts_i = iota((n_ep, rows), 0).astype(F32)
    hits = [(routes[k : k + 1, :] == experts_i).astype(F32) for k in range(2)]
    before = dot(hits[0] + hits[1], upper)
    spread = (lax.shift_right_logical(iota((rows, rows * sub), 1), 3) == iota((rows, rows * sub), 0)).astype(F32)
    lane_row = iota((rows * sub, rows), 1)
    row_of = lax.shift_right_logical(iota((rows * sub, rows), 0), 3)
    gather_col = (lane_row == row_of).astype(F32)
    slot_rows, slot_cols, weight_cols = [], [], []
    for k in range(2):
        slot = routes[k : k + 1, :] * cap_pad + jnp.sum(hits[k] * before, axis=0, keepdims=True)
        slot_rows.append(dot(jnp.broadcast_to(slot, (8, rows)), spread)[0:1])
        slot_cols.append(jnp.sum(gather_col * slot, axis=1, keepdims=True))
        weight_cols.append(jnp.sum(gather_col * rw_v[k : k + 1, :], axis=1, keepdims=True))

    chunk = cap_pad * sub

    def fill_pick(i, carry):
        m = iota((chunk, rows * sub), 0) + i * chunk
        n = iota((chunk, rows * sub), 1)
        slot_m = lax.shift_right_logical(m, 3).astype(F32)
        same = lax.bitwise_and(m, 7) == lax.bitwise_and(n, 7)
        hit = jnp.where(slot_m == slot_rows[0], 1.0, 0.0) + jnp.where(slot_m == slot_rows[1], 1.0, 0.0)
        pick_v[pl.ds(i * chunk, chunk), :] = jnp.where(same, hit, 0.0).astype(BF16)
        return carry

    lax.fori_loop(0, n_ep, fill_pick, 0)
    for k in range(2):
        m = iota((rows * sub, slots * sub), 0)
        n = iota((rows * sub, slots * sub), 1)
        same = lax.bitwise_and(m, 7) == lax.bitwise_and(n, 7)
        hit = jnp.where(lax.shift_right_logical(n, 3).astype(F32) == slot_cols[k], 1.0, 0.0)
        back_v[k] = jnp.where(same, hit, 0.0).astype(BF16)

    wait_bytes(rec1e.at[pl.ds(0, n_tp - 1)], rsem.at[1])
    wait_bytes(rec1.at[pl.ds(0, n_tp - 1)], rsem.at[0])
    ext = rec1e[...][:, 0, :]
    lat_sel = (lax.shift_right_logical(iota((lat_blk, n_tp), 1), per_row.bit_length() - 1) == iota((lat_blk, n_tp), 0)).astype(F32)
    lat_raw = dot(lat_sel.astype(BF16), ext[:, LANES : 2 * LANES].astype(BF16))
    lat_ms = jnp.sum(jnp.sum(lat_raw * lat_raw, axis=1, keepdims=True), axis=0, keepdims=True) / (lat_blk * LANES)
    new_lat = (lat_raw * lax.rsqrt(lat_ms + EPSILON) * lgain_v[...]).astype(BF16)
    nl_v[...] = new_lat
    new_lat_f = new_lat.astype(F32)
    q_pe = rotated(ext[:, 0:64]).astype(BF16)

    def to_blocks(rec, count):
        scat_v[0 : count * lat_blk, :] = rec[...].astype(F32).reshape(count * lat_blk, LANES)
        return [scat_v[pl.ds(j, count, stride=lat_blk), :] for j in range(lat_blk)]

    q_blocks = to_blocks(rec1, n_tp)
    own = q_blocks[0] * new_lat_f[0:1, :]
    for j in range(1, lat_blk):
        own = own + q_blocks[j] * new_lat_f[j : j + 1, :]
    own_score = jnp.sum(own, axis=1, keepdims=True) + jnp.sum(
        q_pe.astype(F32) * new_rope.astype(F32), axis=1, keepdims=True
    )
    own_score = own_score * score_scale
    q_all = jnp.concatenate(q_blocks, axis=1).astype(BF16)
    copies[7].wait()
    copies[8].wait()
    scores = (dot_nt(q_all, cl_v[...]) + dot(q_pe, cr_v[...])) * score_scale
    visible = iota(scores.shape, 1) < len_s[0]
    row_max = jnp.maximum(jnp.max(jnp.where(visible, scores, -jnp.inf), axis=1, keepdims=True), own_score)
    weights = jnp.where(visible, jnp.exp(scores - row_max), 0.0)
    own_weight = jnp.exp(own_score - row_max)
    denominator = jnp.sum(weights, axis=1, keepdims=True) + own_weight
    probs = (weights / denominator).astype(BF16)
    own_prob = (own_weight / denominator).astype(BF16).astype(F32)
    attended = dot(probs, cl_v[...])
    for j in range(lat_blk):
        scat_v[j * n_tp : (j + 1) * n_tp, :] = (
            attended[:, j * LANES : (j + 1) * LANES] + own_prob * new_lat_f[j : j + 1, :]
        )
    for r in range(n_tp):
        msg2[r] = scat_v[pl.ds(r, lat_blk, stride=n_tp), :].astype(BF16)
    rec2[t] = msg2[t]
    send_to_all("tp", n_tp, t, lambda p: msg2.at[p], rec2.at[t], ssem.at[2], rsem.at[2])
    copies[9].wait()
    copies[10].wait()
    wait_bytes(rec2.at[pl.ds(0, n_tp - 1)], rsem.at[2])

    head_lat = jnp.concatenate(to_blocks(rec2, rows), axis=1).astype(BF16)
    values = dot(head_lat, wvu_v[...]).astype(BF16)
    for b in range(nblk):
        scat_v[b * rows : (b + 1) * rows, :] = dot(values, wo_v[:, b * LANES : (b + 1) * LANES])
    for r in range(rows):
        msg3[r] = scat_v[pl.ds(r, nblk, stride=rows), :].astype(BF16)
    rec3[t] = msg3[t]
    send_to_all("tp", n_tp, t, lambda p: msg3.at[p], rec3.at[t], ssem.at[3], rsem.at[3])
    wait_bytes(rec3.at[pl.ds(0, n_tp - 1)], rsem.at[3])

    mixed = rec3[0].astype(F32)
    for r in range(1, n_tp):
        mixed = mixed + rec3[r].astype(F32)

    def block_scale(v):
        total = jnp.sum(jnp.sum(v * v, axis=1, keepdims=True), axis=0, keepdims=True)
        return v * lax.rsqrt(total / (nblk * LANES) + EPSILON)

    resid = (rows_v[0] + block_scale(mixed) * rows_v[1]).astype(BF16).astype(F32)
    expert_in = (block_scale(resid) * rows_v[2]).astype(BF16)
    for c in range(X_SIZE):
        msg4[c] = expert_in[c * sub : (c + 1) * sub, :]
    rec4[t] = msg4[x]
    send_to_all("tp", n_tp, t, lambda p: msg4.at[lax.rem(p, X_SIZE)], rec4.at[t], ssem.at[4], rsem.at[4])
    wait_bytes(rec4.at[pl.ds(0, n_tp - 1)], rsem.at[4])

    own_cols = rec4[...].astype(F32).reshape(rows * sub, LANES).astype(BF16)
    msg5[...] = dot(pick_v[...], own_cols).astype(BF16).reshape(n_ep, chunk, LANES)
    rec5[e] = msg5[e]
    send_to_all("ep", n_ep, e, lambda p: msg5.at[p], rec5.at[e], ssem.at[5], rsem.at[5])
    packed = chunks6.shape[1]
    sel_slot = iota((packed, slots), 1)
    sel_group = jnp.floor((sel_slot.astype(F32) + 0.5) * (1.0 / cap_pad))
    sel_in = sel_slot.astype(F32) - cap_pad * sel_group
    sel_row = iota((packed, slots), 0).astype(F32)
    select = jnp.where((sel_row == sel_group * cap + sel_in) & (sel_in < cap), 1.0, 0.0).astype(BF16)
    exp_slot = iota((slots, packed), 0).astype(F32)
    exp_group = jnp.floor((exp_slot + 0.5) * (1.0 / cap_pad))
    exp_in = exp_slot - cap_pad * exp_group
    exp_row = iota((slots, packed), 1).astype(F32)
    expand = jnp.where((exp_row == exp_group * cap + exp_in) & (exp_in < cap), 1.0, 0.0).astype(BF16)
    wait_bytes(rec5.at[pl.ds(0, n_ep - 1)], rsem.at[5])

    scat_v[0 : slots * sub, :] = rec5[...].astype(F32).reshape(slots * sub, LANES)
    for j in range(sub):
        block = scat_v[pl.ds(j, slots, stride=sub), :].astype(BF16)
        chunks6[x, :, j * LANES : (j + 1) * LANES] = dot(select, block).astype(BF16)

    def x_copy(i, source, target, ss, rs):
        return pltpu.make_async_remote_copy(
            src_ref=source,
            dst_ref=target,
            send_sem=ss,
            recv_sem=rs,
            device_id={"tp": y0 + lax.rem(x + i, X_SIZE)},
            device_id_type=pl.DeviceIdType.MESH,
        )

    for i in range(1, X_SIZE):
        x_copy(i, chunks6.at[x], chunks6.at[x], ssem.at[6 + i], rsem6.at[i]).start()
    copies[11].wait()
    copies[12].wait()
    width = sub * LANES

    def project(c):
        return dot_nt(chunks6[c], wgu_v[:, pl.ds(pl.multiple_of(c * width, width), width)])

    sums = project(x)
    for i in (1, 3, 2):
        c = lax.rem(x + X_SIZE - i, X_SIZE)
        wait_bytes(chunks6.at[c], rsem6.at[i])
        sums = sums + project(c)
    gate = sums[:, 0:64]
    hidden = (gate / (1.0 + jnp.exp(-gate)) * sums[:, 64:128]).astype(BF16)
    copies[13].wait()

    def partial(c):
        return dot(hidden, wd_v[:, pl.ds(pl.multiple_of(c * width, width), width)]).astype(BF16)

    for i in (2, 1, 3):
        c = lax.rem(x + i, X_SIZE)
        msg7[i] = partial(c)
        x_copy(i, msg7.at[i], rec7.at[i], ssem.at[9 + i], rsem7.at[i]).start()
    summed = partial(x).astype(F32)
    for i in (1, 3, 2):
        wait_bytes(rec7.at[i], rsem7.at[i])
        summed = summed + rec7[i].astype(F32)
    summed = summed.astype(BF16)
    for j in range(sub):
        scat_v[pl.ds(j, slots, stride=sub), :] = dot(expand, summed[:, j * LANES : (j + 1) * LANES])
    msg8[...] = scat_v[0 : slots * sub, :].astype(BF16).reshape(n_ep, chunk, LANES)
    rec8[e] = msg8[e]
    send_to_all("ep", n_ep, e, lambda p: msg8.at[p], rec8.at[e], ssem.at[13], rsem.at[6])
    wait_bytes(rec8.at[pl.ds(0, n_ep - 1)], rsem.at[6])

    back = rec8[...].reshape(slots * sub, LANES)
    routed = weight_cols[0] * dot(back_v[0], back) + weight_cols[1] * dot(back_v[1], back)
    msg9[...] = routed.reshape(rows, sub, LANES).astype(BF16)
    rec9[t] = msg9[t]
    send_to_all("tp", n_tp, t, lambda p: msg9.at[p], rec9.at[t], ssem.at[14], rsem.at[7])
    wait_bytes(rec9.at[pl.ds(0, n_tp - 1)], rsem.at[7])
    parts = []
    for c in range(X_SIZE):
        part = rec9[c].astype(F32)
        for r in range(c + X_SIZE, n_tp, X_SIZE):
            part = part + rec9[r].astype(F32)
        parts.append(part)
    total = jnp.concatenate(parts, axis=0)
    out_v[...] = (resid + block_scale(total) * rows_v[3]).astype(BF16)

    wait_bytes(msg1.at[pl.ds(0, n_tp - 1)], ssem.at[0])
    wait_bytes(extra1.at[pl.ds(0, n_tp - 1)], ssem.at[1])
    wait_bytes(msg2.at[pl.ds(0, n_tp - 1)], ssem.at[2])
    wait_bytes(msg3.at[pl.ds(0, n_tp - 1)], ssem.at[3])
    wait_bytes(rec4.at[pl.ds(0, n_tp - 1)], ssem.at[4])
    wait_bytes(msg5.at[pl.ds(0, n_ep - 1)], ssem.at[5])
    for i in range(1, X_SIZE):
        wait_bytes(chunks6.at[x], ssem.at[6 + i])
        wait_bytes(msg7.at[i], ssem.at[9 + i])
    wait_bytes(msg8.at[pl.ds(0, n_ep - 1)], ssem.at[13])
    wait_bytes(msg9.at[pl.ds(0, n_tp - 1)], ssem.at[14])


def on_device(
    tokens,
    norm_gains,
    w_query,
    w_query_rope,
    w_key_up,
    w_value_up,
    w_output,
    w_latent_down,
    latent_gain,
    w_rope_down,
    cache_latent,
    cache_rope,
    lengths,
    routes,
    route_weights,
    w_gate,
    w_up,
    w_down,
):
    n_ep = lax.axis_size("ep")
    n_tp = lax.axis_size("tp")
    rows, width = tokens.shape
    nblk = width // LANES
    sub = nblk // X_SIZE
    cap = min(CAP, rows) if rows == 32 else rows
    cap_pad = CAP_PAD if rows == 32 else rows
    slots = n_ep * cap_pad
    packed = -(-n_ep * cap // 16) * 16
    cache = cache_latent.shape[1]
    latent = cache_latent.shape[2]
    nope_width = w_key_up.shape[1]
    rope_width = w_rope_down.shape[1]
    half = rope_width // 2
    frequency = ROTARY_BASE ** (-jnp.arange(half, dtype=F32) / half)
    angles = lengths.astype(F32)[:, None] * frequency
    cos, sin = jnp.cos(angles), jnp.sin(angles)
    trig = jnp.concatenate(
        [jnp.concatenate([cos, cos], axis=1), jnp.concatenate([-sin, sin], axis=1)], axis=0
    )
    swap = functools.partial(jnp.swapaxes, axis1=-1, axis2=-2)
    operands = (
        tokens,
        norm_gains,
        w_query,
        swap(w_query_rope),
        w_key_up,
        w_value_up,
        w_output,
        swap(w_latent_down),
        latent_gain.reshape(latent // LANES, LANES),
        swap(w_rope_down),
        cache_latent,
        swap(cache_rope),
        lengths,
        swap(routes),
        swap(route_weights),
        swap(w_gate),
        swap(w_up),
        w_down,
        trig,
    )
    in_hbm = pl.BlockSpec(memory_space=pl.ANY)
    in_vmem = pl.BlockSpec(memory_space=pltpu.VMEM)
    in_smem = pl.BlockSpec(memory_space=pltpu.SMEM)
    specs = [in_hbm] * len(operands)
    for i in (8, 13, 14, 18):
        specs[i] = in_vmem
    specs[12] = in_smem
    vm = pltpu.VMEM
    chunk = cap_pad * sub
    scratch = [
        vm((rows, width), BF16),
        vm((4, width), F32),
        vm(w_query.shape, BF16),
        vm((2 * rope_width + latent // n_tp, width), BF16),
        vm(w_key_up.shape[1:], BF16),
        vm(w_value_up.shape[1:], BF16),
        vm(w_output.shape, BF16),
        vm((cache, latent), BF16),
        vm((rope_width, cache), BF16),
        vm((128, width), BF16),
        vm(w_down.shape[1:], BF16),
        pltpu.SemaphoreType.DMA((14,)),
        vm((rows, width), BF16),
        vm((4, nblk, LANES), F32),
        vm((max(nblk * rows, slots * sub), LANES), F32),
        vm((n_tp, 1, 2 * LANES), F32),
        vm((n_tp, 8, LANES), BF16),
        vm((n_tp, 1, 2 * LANES), F32),
        vm((n_tp, 8, LANES), BF16),
        vm((n_tp, 8, LANES), BF16),
        vm((n_tp, 8, LANES), BF16),
        vm((n_tp, nblk, LANES), BF16),
        vm((n_tp, nblk, LANES), BF16),
        vm((X_SIZE, sub, LANES), BF16),
        vm((n_tp, sub, LANES), BF16),
        vm((n_ep, chunk, LANES), BF16),
        vm((n_ep, chunk, LANES), BF16),
        vm((X_SIZE, packed, sub * LANES), BF16),
        vm((X_SIZE, packed, sub * LANES), BF16),
        vm((X_SIZE, packed, sub * LANES), BF16),
        vm((n_ep, chunk, LANES), BF16),
        vm((n_ep, chunk, LANES), BF16),
        vm((n_tp, sub, LANES), BF16),
        vm((n_tp, sub, LANES), BF16),
        vm((slots * sub, rows * sub), BF16),
        vm((2, rows * sub, slots * sub), BF16),
        pltpu.SemaphoreType.DMA((15,)),
        pltpu.SemaphoreType.DMA((8,)),
        pltpu.SemaphoreType.DMA((X_SIZE,)),
        pltpu.SemaphoreType.DMA((X_SIZE,)),
    ]
    kernel = functools.partial(
        step_kernel, n_ep, n_tp, cap, cap_pad, (nope_width + rope_width) ** (-0.5)
    )
    hidden, new_latent, new_rope = pl.pallas_call(
        kernel,
        out_shape=(
            jax.ShapeDtypeStruct((nblk, LANES), BF16),
            jax.ShapeDtypeStruct((latent // LANES, LANES), BF16),
            jax.ShapeDtypeStruct((1, rope_width), BF16),
        ),
        in_specs=specs,
        out_specs=(in_vmem, in_vmem, in_vmem),
        scratch_shapes=scratch,
        compiler_params=pltpu.CompilerParams(
            collective_id=0, has_side_effects=True, vmem_limit_bytes=56 << 20
        ),
    )(*operands)
    return hidden.reshape(1, width), new_latent.reshape(1, latent), new_rope


def solution(mesh):
    in_specs = (
        P("ep", None),
        P(),
        P(None, "tp"),
        P(None, "tp"),
        P("tp", None, None),
        P("tp", None, None),
        P("tp", None),
        P(None, "tp"),
        P(),
        P(),
        P(("ep", "tp"), None, None),
        P(("ep", "tp"), None, None),
        P(("ep", "tp")),
        P("ep", None),
        P("ep", None),
        P("ep", None, "tp"),
        P("ep", None, "tp"),
        P("ep", "tp", None),
    )
    out_specs = (P(("ep", "tp"), None), P(("ep", "tp"), None), P(("ep", "tp"), None))
    return jax.shard_map(
        on_device, mesh=mesh, in_specs=in_specs, out_specs=out_specs, check_vma=False
    )
```

time: 289 us -> 118 us (0.41); the launches traced: 286 us -> 118 us
  Pallas kernels: 0 us -> 112 us
  waiting for transfers between devices: 102 us -> 0 us
  blocking collectives: 90.4 us -> 0 us
  starting transfers between devices: 41.2 us -> 0 us
  matrix products: 15.5 us -> 0 us
  other arithmetic: 15.5 us -> 0.75 us
  local copies, waits for them, and re-layouts: 16.8 us -> 3.72 us
  between operations: 4.49 us -> 1.3 us
    pallas_call x0 -> x1, Pallas kernels: none -> 112 us  [on_device(): pl.pallas_call(kernel, out_shape=(jax.ShapeDtypeStruct((nblk, LANES), BF1...]
    all_to_all x7 -> x0, waiting for transfers between devices: 102 us -> none  [the longest x1 56.4 us: on_device(): lax.all_to_all(expert_out, 'ep', split_axis=0, concat_axis=0, tiled=True)]
    all_to_all x2 -> x0, blocking collectives: 90.4 us -> none  [the longest x1 78.6 us: on_device(): lax.all_to_all(outgoing, 'ep', split_axis=0, concat_axis=0, tiled=True)]
    all_to_all x7 -> x0, starting transfers between devices: 41.2 us -> none  [the longest x1 10.5 us: on_device(): lax.all_to_all(latent_cols, 'tp', split_axis=0, concat_axis=1, tiled=True)]
    dot_general x15 -> x0, matrix products: 15.5 us -> none  [the longest x1 3.47 us: on_device(): jnp.dot(hidden_units, w_down[0], preferred_element_type=jnp.float32)]
    all_to_all x7 -> x0, local copies, waits for them, and re-layouts: 8.78 us -> none  [the longest x2 4.2 us: on_device(): lax.all_to_all(expert_out, 'ep', split_axis=0, concat_axis=0, tiled=True)]
    reduce_sum x10 -> x0, other arithmetic: 5.93 us -> none  [the longest x5 4.45 us: rms_scale(): jnp.mean(values_f * values_f, axis=-1, keepdims=True) + EPSILON]
  transfers between devices with their start and end apart: 7 -> 0, of which waited for: 7 -> 0; matrix products, arithmetic and copies ran while one was open for 4% -> 0% of each run, Pallas kernels for 0% -> 0%
where the time goes in v1:
time: 118 us
  Pallas kernels  112 us (95%)
  local copies, waits for them, and re-layouts  3.72 us (3%)
  between operations  1.3 us (1%)
    pallas_call x1, Pallas kernels, on_device(): pl.pallas_call(kernel, out_shape=(jax.ShapeDtypeStruct((nblk, LANES), BF1...  112 us
    unnamed x3, local copies, waits for them, and re-layouts  3.72 us

profile of v1, /device:TPU:1, one launch (start us, length us, event | category | flops | bytes accessed | tf_op | source)
XLA Modules:
  0.0 117.9 jit_solution(9322856623401668511)
XLA Ops:
  1.3 0.1 fusion
  1.3 0.1 fusion.2
  1.4 0.6 maximum_maximum_fusion.trig_v
  2.0 112.1 %shard_map.193 = (bf16[32,128]{1,0:T(8,128)(2,1)}, bf16[8,128]{1,0:T(8,128)(2,1)}, bf16[1,64]{1,0:T(2,128)(2,1)}) custom-call(bf16[32,4096]{1,0:T(8,128)(2,1)} %tokens_h.1, f32[4,4096]{1,0:T(4,128)} %gains_h.1, bf16[4096,128]{1,0:T(8,128)(2,1)} %wq_h.1, bf16[64,4096]{1,0:T(8,128)(2,1)} %bitcast.20, bf16[1,128,1024]{2,1,0:T(8,128)(2,1)} %wku_h.1, ...), custom_call_target="tpu_custom_call" | custom-call | tf_op jit(solution)/shard_map/pallas_call | solution.py:542
  114.1 1.3 %copy.25 = bf16[1,1,32,128]{3,1,2,0:T(2,128)(2,1)} copy(bf16[1,1,32,128]{3,2,1,0:T(8,128)(2,1)} %bitcast.27) | data formatting | bytes 16384
  115.5 1.3 %copy.26 = bf16[1,1,8,128]{3,1,2,0:T(2,128)(2,1)} copy(bf16[1,1,8,128]{3,2,1,0:T(8,128)(2,1)} %bitcast.30) | data formatting | bytes 4096
  116.7 1.1 copy.29
